TPU v7x, 512 devices: a whole 4x4x16 slice. The times are simulated.
512 devices in a mesh: sp: 64 (over z, y), tp: 8 (over x, core).
Axes of the slice: x: 4, y: 4, z: 16, core: 2. Of those that a mesh axis runs over, the one named last changes fastest.
Arguments:
- residual_signal: bfloat16 [16384, 2048], P('sp'), may hold values from -6 to 6
- reading_probe_preactivations: bfloat16 [16384, 1024], P('sp', 'tp'), may hold values from -6 to 6
- keep_switch_preactivations: bfloat16 [16384, 1024], P('sp', 'tp'), may hold values from -5.5 to 5.5
- written_entries: bfloat16 [16384, 1024], P('sp', 'tp'), may hold values from -6 to 6
- emission_switch_preactivations: bfloat16 [16384, 1024], P('sp', 'tp'), may hold values from -6 to 6
- additional_shrink_amount: float32 [16384, 1024], P('sp', 'tp'), may hold values from -0.7 to 0
- complement_of_floor: float32 [1024], P('tp'), may hold values from 6.1035156e-06 to 0.1
- per_group_rescaler: float32 [128], replicated, may hold values from 0.1 to 1.9
- emission_linear_map: bfloat16 [1024, 2048], P('tp'), may hold values from -0.1875 to 0.1875
- channel_layer_rescaler: float32 [2048], replicated, may hold values from 0.1 to 1.9
- expanding_linear_map: bfloat16 [2048, 8192], P('sp', 'tp'), may hold values from -0.125 to 0.125
- contracting_linear_map: bfloat16 [2048, 8192], P('sp', 'tp'), may hold values from -0.0625 to 0.0625
Outputs:
- layer_out: bfloat16 [16384, 2048], P('sp')
All inputs are finite; a program needn't handle non-finite values.
Results may differ from a plain program's by a relative error of at most 0.006.
Values may be sent and summed in bfloat16 or wider, within the bound.
A program may use at most 64 MiB of HBM per device.

v0:
```python
import jax
import jax.numpy as jnp
from jax import lax
from jax.sharding import Mesh
from jax.sharding import PartitionSpec as P

HEAD = 128
BLOCK = 64
SP = ("sp_0", "sp_1")


norm_eps = 1e-06
HIGH_ACCURACY = lax.Precision.HIGHEST


def filled_with(shard, identity):
    return jax.tree.map(
        lambda a, e: jnp.broadcast_to(jnp.asarray(e, a.dtype), a.shape), shard, identity
    )


def gathered_once(shard, axis):
    leaves = jax.tree.leaves(shard)
    turns = sorted(range(len(leaves)), key=lambda k: -leaves[k].size)
    width = (1, *leaves[turns[0]].shape)[-1]
    lines = [
        jnp.pad(leaves[k].reshape(-1), (0, -leaves[k].size % width)).reshape(-1, width)
        for k in turns
    ]
    both, at, found = (lax.all_gather(jnp.concatenate(lines), axis), 0, {})
    for k, line in zip(turns, lines):
        piece = both[:, at : at + len(line)].reshape(len(both), -1)
        found[k] = piece[:, : leaves[k].size].reshape(-1, *leaves[k].shape)
        at += len(line)
    numbers = iter(range(len(leaves)))
    return jax.tree.map(lambda _: found[next(numbers)], shard)


def entering(shard, axes, combine, identity):
    before = start = filled_with(shard, identity)
    total = shard
    for axis in reversed(axes):
        peers, index = (lax.axis_size(axis), lax.axis_index(axis))
        pieces = gathered_once(total, axis)
        inside, total = (start, start)
        for k in range(peers):
            passed = k < index
            total = combine(total, jax.tree.map(lambda part: part[k], pieces))
            inside = jax.tree.map(lambda new, old: jnp.where(passed, new, old), total, inside)
        before = combine(inside, before)
    return before


def laid_out(blocks, dim):
    lengths = list(blocks.shape[1:])
    lengths[dim] *= blocks.shape[0]
    return jnp.moveaxis(blocks, 0, dim).reshape(lengths)


def copy_for_each(shard, axis):
    peers = lax.axis_size(axis)
    return lax.all_to_all(
        jnp.broadcast_to(shard[None], (peers, *shard.shape)), axis, 0, 0, tiled=True
    )


def gathered_copies(shard, axis, dim):
    return laid_out(copy_for_each(shard, axis), dim)


def in_one_piece(arrays, axis, dim, along):
    widths = [a.shape[along] for a in arrays]
    both = jnp.concatenate(arrays, axis=along)
    whole = lax.all_gather(both, axis, axis=dim, tiled=True)
    return tuple(jnp.split(whole, [sum(widths[:k]) for k in range(1, len(widths))], axis=along))


def cut_along(shard, dim, peers):
    lengths = shard.shape
    blocks = shard.reshape(*lengths[:dim], peers, lengths[dim] // peers, *lengths[dim + 1 :])
    return jnp.moveaxis(blocks, dim, 0)


def sum_at_owner(shard, axis, dim):
    blocks = cut_along(shard, dim, lax.axis_size(axis))
    arrived = lax.all_to_all(blocks, axis, split_axis=0, concat_axis=0, tiled=True)
    return arrived.astype(jnp.float32).sum(axis=0)


def block_step(state_matrix, inputs):
    query_block_rows, key_blk, logs_blk, value_block_rows = inputs
    cumulative_decay = jnp.cumsum(logs_blk, axis=1)
    carried_state = jnp.einsum(
        "rlb,rbz->rlz",
        query_block_rows * jnp.exp(cumulative_decay),
        state_matrix,
        precision=HIGH_ACCURACY,
    )
    spread = cumulative_decay[:, :, None, :] - cumulative_decay[:, None, :, :]
    places = jnp.arange(BLOCK)
    lower = places[:, None] >= places[None, :]
    decay = jnp.exp(jnp.where(lower[None, :, :, None], spread, -jnp.inf))
    scores = jnp.einsum(
        "htk,hsk,htsk->hts", query_block_rows, key_blk, decay, precision=HIGH_ACCURACY
    )
    result = carried_state + jnp.einsum(
        "hts,hsv->htv", scores, value_block_rows, precision=HIGH_ACCURACY
    )
    final_state = cumulative_decay[:, -1:, :]
    decayed_key_rows = key_blk * jnp.exp(final_state - cumulative_decay)
    state_matrix = jnp.exp(final_state[:, 0, :])[..., None] * state_matrix + jnp.einsum(
        "aux,auf->axf", decayed_key_rows, value_block_rows, precision=HIGH_ACCURACY
    )
    return (state_matrix, result)


def combine_carry(earlier, later):
    return (earlier[0] * later[0], later[0][..., None] * earlier[1] + later[1])


def body(
    residual_signal,
    reading_probe_preactivations,
    keep_switch_preactivations,
    written_entries,
    emission_switch_preactivations,
    additional_shrink_amount,
    complement_of_floor,
    per_group_rescaler,
    emission_linear_map,
    channel_layer_rescaler,
    expanding_linear_map,
    contracting_linear_map,
):
    positions = reading_probe_preactivations.shape[0]
    channels = reading_probe_preactivations.shape[1]
    local_heads = channels // HEAD
    count = positions // BLOCK
    query_act = jax.nn.silu(reading_probe_preactivations.astype(jnp.float32))
    logarithmic_keep_fraction = (
        jnp.logaddexp(
            jnp.log1p(-complement_of_floor),
            jnp.log(complement_of_floor)
            + jax.nn.log_sigmoid(keep_switch_preactivations.astype(jnp.float32)),
        )
        + additional_shrink_amount
    )
    key_part = -jnp.expm1(logarithmic_keep_fraction)
    value_part = written_entries.astype(jnp.float32)

    def to_blocks(values):
        return values.reshape(count, BLOCK, local_heads, HEAD).transpose(0, 2, 1, 3)

    start = jnp.zeros((local_heads, HEAD, HEAD), jnp.float32)
    state_end, outputs = lax.scan(
        block_step,
        start,
        (
            to_blocks(query_act),
            to_blocks(key_part),
            to_blocks(logarithmic_keep_fraction),
            to_blocks(value_part),
        ),
    )
    within_block_output = outputs.transpose(0, 2, 1, 3).reshape(positions, local_heads, HEAD)
    running = jnp.cumsum(logarithmic_keep_fraction, axis=0)
    decay_total = jnp.exp(running[-1]).reshape(local_heads, HEAD)
    identity = (
        jnp.ones((local_heads, HEAD), jnp.float32),
        jnp.zeros((local_heads, HEAD, HEAD), jnp.float32),
    )
    prior_state = entering((decay_total, state_end), SP, combine_carry, identity)
    weighted_scores = (query_act * jnp.exp(running)).reshape(positions, local_heads, HEAD)
    recurrent_output = within_block_output + jnp.einsum(
        "pnm,nmx->pnx", weighted_scores, prior_state[1], precision=HIGH_ACCURACY
    )
    scaled = (
        recurrent_output
        * lax.rsqrt(
            jnp.mean(recurrent_output * recurrent_output, axis=-1, keepdims=True) + norm_eps
        )
        * per_group_rescaler
    )
    gated = scaled * jax.nn.silu(emission_switch_preactivations.astype(jnp.float32)).reshape(
        positions, local_heads, HEAD
    )
    mixed_heads = gated.reshape(positions, channels).astype(jnp.bfloat16)
    all_heads = gathered_copies(mixed_heads, "tp", 1)
    full_out = lax.all_gather(emission_linear_map, "tp", axis=0, tiled=True)
    projected = jnp.dot(all_heads, full_out, preferred_element_type=jnp.float32)
    after_mix = residual_signal.astype(jnp.float32) + projected
    normed = (
        after_mix
        * lax.rsqrt(jnp.mean(after_mix * after_mix, axis=-1, keepdims=True) + norm_eps)
        * channel_layer_rescaler
    ).astype(jnp.bfloat16)
    up_whole, down_whole = in_one_piece((expanding_linear_map, contracting_linear_map), SP, 0, 1)
    upward = jnp.dot(normed, up_whole, preferred_element_type=jnp.float32)
    hidden = jnp.square(jax.nn.relu(upward)).astype(jnp.bfloat16)
    share = positions // lax.axis_size("tp")
    downward = sum_at_owner(
        lax.dot_general(
            hidden, down_whole, (((1,), (1,)), ((), ())), preferred_element_type=jnp.float32
        ).astype(jnp.bfloat16),
        "tp",
        0,
    )
    own_start = lax.axis_index("tp") * share
    own_mix = lax.dynamic_slice_in_dim(after_mix, own_start, share, 0)
    finished = (own_mix + downward).astype(jnp.bfloat16)
    return gathered_copies(finished, "tp", 0)


def solution(mesh):
    finer = Mesh(mesh.devices.reshape(16, 4, mesh.shape["tp"]), ("sp_0", "sp_1", "tp"))
    return jax.shard_map(
        body,
        mesh=finer,
        in_specs=(
            P(SP, None),
            P(SP, "tp"),
            P(SP, "tp"),
            P(SP, "tp"),
            P(SP, "tp"),
            P(SP, "tp"),
            P("tp"),
            P(),
            P("tp", None),
            P(),
            P(SP, "tp"),
            P(SP, "tp"),
        ),
        out_specs=P(SP, None),
        check_vma=False,
    )
```

profile of v0, /device:TPU:1, one launch (start us, length us, event | category | flops | bytes accessed | tf_op | source)
XLA Modules:
  0.0 363.2 jit_solution(13176499211492240413)
XLA Ops:
  6.5 0.7 negate_log-plus-one_fusion
  7.2 1.1 exponential-minus-one_negate_fusion
  8.4 0.1 fusion.63
  8.6 0.1 copy.45
  8.9 1.0 copy.41
  10.1 13.1 %while.13 = (s32[]{:T(128)}, f32[1,128,128]{2,1,0:T(8,128)S(1)}, f32[4,1,64,128]{3,2,1,0:T(8,128)S(1)}, f32[4,1,64,128]{3,2,1,0:T(8,128)S(1)}, f32[4,1,64,128]{3...) while((s32[]{:T(128)}, f32[1,128,128]{2,1,0:T(8,128)S(1)}, ...), condition=%wide.region_2.3_spmd.clone, body=%wide.region_0.2_spmd.clone.sunk | while | flops 34693120 | bytes 5108864 | solution.py:155
  10.1 0.1 reduce_window_sum.34
  10.2 0.6 select_exponential_fusion.2
  10.8 1.7 fusion.174
  12.6 0.2 fusion.173
  12.7 0.2 fusion.175
  13.0 0.3 fusion.172
  13.4 0.1 reduce_window_sum.34
  13.5 0.6 select_exponential_fusion.2
  14.1 1.7 fusion.174
  15.8 0.2 fusion.173
  16.0 0.2 fusion.175
  16.3 0.3 fusion.172
  16.7 0.6 select_exponential_fusion.2
  17.4 1.7 fusion.174
  19.1 0.2 fusion.173
  19.3 0.2 fusion.175
  19.5 0.3 fusion.172
  20.0 0.6 select_exponential_fusion.2
  20.6 1.7 fusion.174
  22.4 0.2 fusion.173
  22.5 0.2 fusion.175
  22.8 0.3 fusion.172
  23.2 10.7 %all-gather.2 = f32[4,129,128]{2,1,0:T(8,128)S(1)} all-gather(f32[1,129,128]{2,1,0:T(8,128)S(1)} %maximum_bitcast_fusion), channel_id=2, replica_groups=mesh['sp_0'=16,'sp_1'=4,'tp'=8] {'sp_1'}, dimensions={0}, use_global_device_ids=true | all-gather | bytes 330240 | tf_op jit(solution)/shard_map/all_gather | solution.py:30
  33.9 0.1 fusion.153
  34.1 0.6 maximum_bitcast_fusion.1
  34.8 0.7 all-gather.8.cloned.1.call-update
  35.6 0.7 pad_maximum_fusion
  36.4 0.1 copy.48
  36.5 65.5 %all-gather.12.cloned.1.call-done = f32[16,129,128]{2,1,0:T(8,128)} async-done(((f32[1,129,128]{2,1,0:T(8,128)}), f32[16,129,128]{2,1,0:T(8,128)}) %all-gather.12.cloned.1.call-update) | async-done | bytes 1056784 | tf_op jit(solution)/shard_map/all_gather | solution.py:30
  102.1 0.8 slice_bitcast_fusion.16
  102.8 2.1 multiply_reduce_fusion.1
  105.1 24.3 %all_to_all.15 = bf16[8,256,128]{1,2,0:T(8,128)(2,1)S(1)} all-to-all(bf16[8,256,128]{1,2,0:T(8,128)(2,1)S(1)} %broadcast_in_dim.32), channel_id=1, replica_groups=mesh['sp_0'=16,'sp_1'=4,'tp'=8] {'tp'}, dimensions={0} | all-to-all | bytes 1048576 | tf_op jit(solution)/shard_map/all_to_all | solution.py:62
  129.4 22.2 %all-gather.8.cloned.1.call-done = bf16[1024,2048]{1,0:T(8,128)(2,1)} async-done(((bf16[128,2048]{1,0:T(8,128)(2,1)}), bf16[1024,2048]{1,0:T(8,128)(2,1)}) %all-gather.8.cloned.1.call-update) | async-done | bytes 4194320 | tf_op jit(solution)/shard_map/all_gather | solution.py:189
  151.7 3.9 %multiply_reduce_fusion = (f32[256]{0:T(256)S(1)}, f32[256,2048]{1,0:T(8,128)S(1)}) fusion(bf16[256,1024]{0,1:T(8,128)(2,1)S(1)} %bitcast.218, bf16[1024,2048]{1,0:T(8,128)(2,1)} %all-gather.8.cloned.1.call-done, bf16[256,2048]{1,0:T(8,128)(2,1)} %param.14), kind=kOutput, calls=%fused_computation.45 | convolution fusion | flops 1075838720 | bytes 7865344 | tf_op jit(solution)/shard_map/dot_general | solution.py:190
  155.5 147.1 %all-gather.10.cloned.1.call-done = bf16[2048,2048]{1,0:T(8,128)(2,1)} async-done(((bf16[32,2048]{1,0:T(8,128)(2,1)}), bf16[2048,2048]{1,0:T(8,128)(2,1)}) %all-gather.10.cloned.1.call-update) | async-done | bytes 8388624 | tf_op jit(solution)/shard_map/all_gather | solution.py:74
  302.7 6.8 %fusion.32 = bf16[256,2048]{1,0:T(8,128)(2,1)} fusion(bf16[2048,2048]{1,0:T(8,128)(2,1)} %all-gather.10.cloned.1.call-done, f32[256,2048]{1,0:T(8,128)S(1)} %get-tuple-element.142, f32[2048]{0:T(1024)S(1)} %copy-done.5, f32[256]{0:T(256)S(1)} %add_rsqrt_fusion), kind=kOutput, calls=%fused_computation.42 | convolution fusion | flops 2150367232 | bytes 11543552 | tf_op jit(solution)/shard_map/dot_general | solution.py:202
  309.5 12.7 %all-to-all-start.1 = ((bf16[8,32,2048]{2,1,0:T(8,128)(2,1)}), bf16[8,32,2048]{2,1,0:T(8,128)(2,1)S(1)}, u32[]{:S(2)}, u32[]{:S(2)}) async-start(bf16[8,32,2048]{2,1,0:T(8,128)(2,1)} %bitcast.223), calls=%async_computation.1 | async-start | bytes 2097152 | tf_op jit(solution)/shard_map/all_to_all | solution.py:86
  322.2 15.0 %all-to-all-done.1 = bf16[8,32,2048]{2,1,0:T(8,128)(2,1)S(1)} async-done(((bf16[8,32,2048]{2,1,0:T(8,128)(2,1)}), bf16[8,32,2048]{2,1,0:T(8,128)(2,1)S(1)}, u32[]{:S(2)}, u32[]{:S(2)}) %all-to-all-start.1) | async-done | bytes 1048608 | tf_op jit(solution)/shard_map/all_to_all | solution.py:86
  337.1 0.1 convert_reduce_fusion
  337.3 0.1 broadcast_in_dim.33
  337.4 18.3 %all_to_all.16 = bf16[8,32,2048]{2,1,0:T(8,128)(2,1)S(1)} all-to-all(bf16[8,32,2048]{2,1,0:T(8,128)(2,1)S(1)} %broadcast_in_dim.33), channel_id=1, replica_groups=mesh['sp_0'=16,'sp_1'=4,'tp'=8] {'tp'}, dimensions={0} | all-to-all | bytes 2097152 | tf_op jit(solution)/shard_map/all_to_all | solution.py:62
  355.7 1.0 copy.80
  (62 shorter events, 1.2 us)
Async XLA Ops:
  6.5 3.5 copy-start
  6.5 95.5 %all-gather.12.cloned.1.call-start = ((), (), s32[]{:S(2)}) async-start(), calls=%async_computation.5 | async-start | bytes 1183744 | tf_op jit(solution)/shard_map/all_gather | solution.py:30
  10.0 25.5 %copy-start.2 = (bf16[32,1024]{1,0:T(8,128)(2,1)S(1)}, bf16[32,1024]{1,0:T(8,128)(2,1)}, u32[]{:S(2)}) copy-start(bf16[32,1024]{1,0:T(8,128)(2,1)} %param.25) | copy-start | bytes 196612
  10.1 25.5 %copy-start.3 = (bf16[32,1024]{1,0:T(8,128)(2,1)S(1)}, bf16[32,1024]{1,0:T(8,128)(2,1)}, u32[]{:S(2)}) copy-start(bf16[32,1024]{1,0:T(8,128)(2,1)} %param.24) | copy-start | bytes 196612
  23.1 13.3 %copy-start.1 = (bf16[256,128]{1,0:T(8,128)(2,1)S(1)}, bf16[256,128]{1,0:T(8,128)(2,1)}, u32[]{:S(2)}) copy-start(bf16[256,128]{1,0:T(8,128)(2,1)} %param.18) | copy-start | bytes 196612
  34.7 70.2 %copy-start.4 = (f32[128]{0:T(128)S(1)}, f32[128]{0:T(128)}, u32[]{:S(2)}) copy-start(f32[128]{0:T(128)} %param.21) | copy-start | bytes 1540
  34.7 116.9 %all-gather.8.cloned.1.call-start = ((), (), s32[]{:S(2)}) async-start(), calls=%async_computation.3 | async-start | bytes 4718592 | tf_op jit(solution)/shard_map/all_gather | solution.py:189
  35.5 267.2 %all-gather.10.cloned.1.call-start = ((), (), s32[]{:S(2)}) async-start(), calls=%async_computation.4 | async-start | bytes 8519680 | tf_op jit(solution)/shard_map/all_gather | solution.py:74
  151.7 151.0 %copy-start.5 = (f32[2048]{0:T(1024)S(1)}, f32[2048]{0:T(1024)}, u32[]{:S(2)}) copy-start(f32[2048]{0:T(1024)} %param.23) | copy-start | bytes 24580
  309.5 27.6 %all-to-all-start.1 = ((bf16[8,32,2048]{2,1,0:T(8,128)(2,1)}), bf16[8,32,2048]{2,1,0:T(8,128)(2,1)S(1)}, u32[]{:S(2)}, u32[]{:S(2)}) async-start(bf16[8,32,2048]{2,1,0:T(8,128)(2,1)} %bitcast.223), calls=%async_computation.1 | async-start | bytes 2097152 | tf_op jit(solution)/shard_map/all_to_all | solution.py:86
Sparse Core Ops, SparseCore 0:
  34.8 67.1 all-gather.11
  104.2 47.3 all-gather.7
  154.6 148.0 all-gather.9
where the time goes:
time: 364 us; the launch traced here: 363 us
  waiting for transfers between devices  251 us (69%)
  blocking collectives  53.4 us (15%)
  matrix products  15.7 us (4%)
  other arithmetic  14.3 us (4%)
  between operations  13.4 us (4%)
  starting transfers between devices  12.8 us (4%)
    all_gather x1, waiting for transfers between devices, in_one_piece(): whole = lax.all_gather(both, axis, axis=dim, tiled=True)  147 us
    all_gather x1, waiting for transfers between devices, gathered_once(): both, at, found = (lax.all_gather(jnp.concatenate(lines), axis), 0, {})  65.5 us
    all_to_all x2, blocking collectives, copy_for_each(): lax.all_to_all(jnp.broadcast_to(shard[None], (peers, *shard.shape)), axis...  42.6 us
    all_gather x1, waiting for transfers between devices, body(): full_out = lax.all_gather(emission_linear_map, 'tp', axis=0, tiled=True)  22.2 us
    all_to_all x1, waiting for transfers between devices, sum_at_owner(): lax.all_to_all(blocks, axis, split_axis=0, concat_axis=0, tiled=True)  15 us
    all_to_all x1, starting transfers between devices, sum_at_owner(): lax.all_to_all(blocks, axis, split_axis=0, concat_axis=0, tiled=True)  12.7 us
    all_gather x1, blocking collectives, gathered_once(): both, at, found = (lax.all_gather(jnp.concatenate(lines), axis), 0, {})  10.7 us
  transfers between devices with their start and end apart: 4, of which 4 were waited for; matrix products, arithmetic and copies ran while one was open for 2% of the time, Pallas kernels for 0%

commit v1 on v0

v1 whole, which is shorter than its diff:
```python
import jax
import jax.numpy as jnp
from jax import lax
from jax.experimental import pallas as pl
from jax.experimental.pallas import tpu as pltpu
from jax.sharding import Mesh
from jax.sharding import PartitionSpec as P

Z, Y, X, C = 16, 4, 4, 2
HEAD = 128
BLOCK = 64
ROWS = 256
D = 2048
MIX = 1024
HID = 1024
NA = 384
NB = HID - NA
SP_N = Z * Y
WR = D // SP_N
STEPS = Z // 2
HALVES = 2
HW = D // HALVES
F32 = jnp.float32
BF16 = jnp.bfloat16
EPS = 1e-06
EXACT = lax.Precision.HIGHEST
NT = (((1,), (1,)), ((), ()))
TN = (((0,), (0,)), ((), ()))


def sigmoid(x):
    return 1.0 / (1.0 + jnp.exp(-x))


def log_one_minus(u):
    series = jnp.zeros_like(u)
    for k in range(9, 0, -1):
        series = u * (1.0 / k + series)
    return jnp.where(u < 0.125, -series, jnp.log(1.0 - u))


def one_minus_exp(w):
    series = jnp.ones_like(w)
    for k in range(10, 1, -1):
        series = 1.0 + (w * (1.0 / k)) * series
    return jnp.where(w > -0.5, -w * series, 1.0 - jnp.exp(w))


def kernel(
    resid,
    read_pre,
    keep_pre,
    written,
    emit_pre,
    shrink,
    floor_c,
    head_gain,
    wout_in,
    norm_gain,
    up_in,
    down_in,
    out,
    wa,
    wb,
    wo,
    after,
    after_scale,
    normed,
    hid_a,
    hid_b,
    heads,
    local_out,
    q_decay,
    mixed,
    ybuf,
    zsend,
    zbuf,
    pbuf,
    pair_out,
    pair_in,
    own_sum,
    rs_out,
    rs_in,
    fin,
    lsem,
    a1_s,
    a1_r,
    a2_s,
    a2_r,
    b1_s,
    b1_r,
    yf_s,
    yf_r,
    yh_s,
    yh_r,
    st_s,
    st_r,
    zs_s,
    zs_r,
    pq_s,
    pq_r,
    wx_s,
    wx_r,
    wc_s,
    wc_r,
    hx_s,
    hx_r,
    hc_s,
    hc_r,
    pp_s,
    pp_r,
    rs_s,
    rs_r,
    gx_s,
    gx_r,
    gc_s,
    gc_r,
):
    z = lax.axis_index("z")
    y = lax.axis_index("y")
    x = lax.axis_index("x")
    c = lax.axis_index("c")
    tp = x * C + c

    def zi(d):
        return lax.rem(z + (d + Z), Z)

    def yi(d):
        return lax.rem(y + (d + Y), Y)

    def xi(d):
        return lax.rem(x + (d + X), X)

    def dev(**kw):
        at = {"z": z, "y": y, "x": x, "c": c}
        at.update(kw)
        return (at["z"], at["y"], at["x"], at["c"])

    def rdma(src, dst, s, r, to):
        return pltpu.make_async_remote_copy(
            src_ref=src,
            dst_ref=dst,
            send_sem=s,
            recv_sem=r,
            device_id=to,
            device_id_type=pl.DeviceIdType.MESH,
        )

    sent = []

    def send(src, dst, s, r, to):
        cp = rdma(src, dst, s, r, to)
        cp.start()
        sent.append(cp)

    def arrive(ref, s, r):
        rdma(ref, ref, s, r, dev(c=1 - c)).wait_recv()

    bar = pltpu.get_barrier_semaphore()
    peers = [dev(z=zi(d)) for d in range(1, Z)]
    peers += [dev(y=yi(d)) for d in range(1, Y)]
    peers += [dev(x=xi(d)) for d in range(1, X)]
    peers += [dev(c=1 - c)]
    for p in peers:
        pl.semaphore_signal(bar, inc=1, device_id=p, device_id_type=pl.DeviceIdType.MESH)

    def rows32(zk, yk, n=WR, off=0):
        return pl.ds(pl.multiple_of((zk * Y + yk) * WR + off, 16), n)

    def a_own():
        return rows32(z, y)

    local = []
    for u, src in ((0, up_in), (1, down_in)):
        local.append(
            pltpu.make_async_copy(src.at[:, pl.ds(0, NA)], wa.at[u, a_own()], lsem.at[2 * u])
        )
        local.append(
            pltpu.make_async_copy(src.at[:, pl.ds(NA, NB)], wb.at[u, a_own()], lsem.at[2 * u + 1])
        )

    def orows(xk, ck, n=HEAD, off=0):
        return pl.ds(pl.multiple_of((xk * C + ck) * HEAD + off, 64), n)

    local.append(pltpu.make_async_copy(wout_in, wo.at[orows(x, c)], lsem.at[4]))
    for cp in local:
        cp.start()

    floor = floor_c[...]
    pre = keep_pre[...].astype(F32)
    logs = log_one_minus(floor * (1.0 / (1.0 + jnp.exp(pre)))) + shrink[...]
    key = one_minus_exp(logs)
    rp = read_pre[...].astype(F32)
    query = rp * sigmoid(rp)
    value = written[...].astype(F32)
    ti = lax.broadcasted_iota(jnp.int32, (BLOCK, BLOCK), 0)
    si = lax.broadcasted_iota(jnp.int32, (BLOCK, BLOCK), 1)
    lower = ti >= si
    tri = lower.astype(F32)
    state = jnp.zeros((HEAD, HEAD), F32)
    base = jnp.zeros((1, HEAD), F32)
    parts = []
    for k in range(ROWS // BLOCK):
        sl = slice(k * BLOCK, (k + 1) * BLOCK)
        lc = jnp.dot(tri, logs[sl], precision=EXACT, preferred_element_type=F32)
        end = lc[BLOCK - 1 :, :]
        kd = key[sl] * jnp.exp(end - lc)
        parts.append((sl, lc, state))
        q_decay[sl, :] = query[sl] * jnp.exp(lc + base)
        state = jnp.exp(end) * state + lax.dot_general(
            value[sl], kd, TN, precision=EXACT, preferred_element_type=F32
        )
        base = base + end
    decay = jnp.exp(base)

    def two_parts(a):
        hi = a.astype(BF16)
        lo = (a - hi.astype(F32)).astype(BF16)
        r = lax.broadcasted_iota(jnp.int32, (16, HEAD), 0)
        both = jnp.where(r == 0, hi.astype(F32), jnp.where(r == 1, lo.astype(F32), 0.0))
        return both.astype(BF16)

    ybuf[y, 0:HEAD, :] = state.astype(BF16)
    ybuf[y, HEAD : HEAD + 16, :] = two_parts(decay)

    for cp in local:
        cp.wait()
    pl.semaphore_wait(bar, len(peers))

    for d in range(1, Y):
        send(ybuf.at[y], ybuf.at[y], st_s.at[d], st_r.at[d], dev(y=yi(d)))
    for u in range(2):
        for d in range(1, Y):
            ref = wa.at[u, a_own()]
            send(ref, ref, a1_s.at[u, d], a1_r.at[u, d], dev(y=yi(d)))

    def send_b(i, step, zk):
        for u in range(2):
            ref = wb.at[u, rows32(zk, y)]
            send(ref, ref, b1_s.at[i, u, step], b1_r.at[i, u, step], dev(z=zi(1 - 2 * i)))

    def send_y(k, zk):
        for u in range(2):
            ref = wb.at[u, rows32(zk, y)]
            for i in range(2):
                send(ref, ref, yf_s.at[i, u, k], yf_r.at[i, u, k], dev(y=yi(1 - 2 * i)))

    def relay_y(k, zk):
        for u in range(2):
            for i in range(2):
                yk = yi(2 * i - 1)
                arrive(wb.at[u, rows32(zk, yk)], yf_s.at[i, u, k], yf_r.at[i, u, k])
                ref = wb.at[u, rows32(zk, yk, 16, 16 * i)]
                send(ref, ref, yh_s.at[i, u, k], yh_r.at[i, u, k], dev(y=yi(1 - 2 * i)))

    def end_y(k, zk):
        for u in range(2):
            for i in range(2):
                ref = wb.at[u, rows32(zk, yi(2), 16, 16 * i)]
                arrive(ref, yh_s.at[i, u, k], yh_r.at[i, u, k])

    def group(zk):
        return pl.ds(pl.multiple_of(zk * (Y * WR), Y * WR), Y * WR)

    def send_a(i, step, zk):
        for u in range(2):
            ref = wa.at[u, group(zk)]
            send(ref, ref, a2_s.at[i, u, step], a2_r.at[i, u, step], dev(z=zi(1 - 2 * i)))

    for i in range(2):
        send_b(i, 1, z)
    own_wo = wo.at[orows(x, c)]
    for i in range(2):
        send(own_wo, own_wo, wx_s.at[i], wx_r.at[i], dev(x=xi(1 - 2 * i)))
    send(own_wo, own_wo, wc_s.at[0], wc_r.at[0], dev(c=1 - c))
    send_y(0, z)

    for sl, lc, st in parts:
        qd = query[sl] * jnp.exp(lc)
        kd = key[sl] * jnp.exp(-lc)
        scores = lax.dot_general(qd, kd, NT, precision=EXACT, preferred_element_type=F32)
        scores = jnp.where(lower, scores, 0.0)
        local_out[sl, :] = jnp.dot(
            scores, value[sl], precision=EXACT, preferred_element_type=F32
        ) + lax.dot_general(qd, st, NT, precision=EXACT, preferred_element_type=F32)

    for u in range(2):
        for d in range(1, Y):
            arrive(wa.at[u, rows32(z, yi(-d))], a1_s.at[u, d], a1_r.at[u, d])
    for i in range(2):
        send_a(i, 1, z)

    def decay_of(block):
        return block[0:1, :].astype(F32) + block[1:2, :].astype(F32)

    for d in range(1, Y):
        arrive(ybuf.at[yi(-d)], st_s.at[d], st_r.at[d])
    quarter = pl.ds(pl.multiple_of(y * (HEAD // Y), HEAD // Y), HEAD // Y)
    row_q = jnp.zeros((HEAD // Y, HEAD), F32)
    row_a = jnp.ones((1, HEAD), F32)
    for k in range(Y):
        a_k = decay_of(ybuf[k, HEAD : HEAD + 16, :])
        row_q = a_k * row_q + ybuf[k, quarter, :].astype(F32)
        row_a = row_a * a_k
    zsend[0 : HEAD // Y, :] = row_q.astype(BF16)
    zsend[HEAD // Y : HEAD // Y + 16, :] = two_parts(row_a)
    for d in range(1, Z):

        @pl.when(z + d < Z)
        def _():
            rdma(zsend, zbuf.at[z], zs_s.at[d], zs_r.at[d], dev(z=zi(d))).start()

    def stage_wout():
        for i in range(2):
            xk = xi(2 * i - 1)
            full = wo.at[orows(xk, c)]
            arrive(full, wx_s.at[i], wx_r.at[i])
            half = wo.at[orows(xk, c, 64, 64 * i)]
            send(half, half, wx_s.at[2 + i], wx_r.at[2 + i], dev(x=xi(1 - 2 * i)))
            send(full, full, wc_s.at[1 + i], wc_r.at[1 + i], dev(c=1 - c))

    def stage_wout2():
        for i in range(2):
            half = wo.at[orows(xi(2), c, 64, 64 * i)]
            arrive(half, wx_s.at[2 + i], wx_r.at[2 + i])
            send(half, half, wc_s.at[3 + i], wc_r.at[3 + i], dev(c=1 - c))

    def stage_z():
        for d in range(1, Z):

            @pl.when(z - d >= 0)
            def _():
                arrive(zbuf.at[zi(-d)], zs_s.at[d], zs_r.at[d])

        def add(k, acc):
            a_k = decay_of(zbuf[k, HEAD // Y : HEAD // Y + 16, :])
            return a_k * acc + zbuf[k, 0 : HEAD // Y, :].astype(F32)

        pbuf[quarter, :] = lax.fori_loop(0, z, add, jnp.zeros((HEAD // Y, HEAD), F32))
        for d in range(1, Y):
            ref = pbuf.at[quarter]
            send(ref, ref, pq_s.at[d], pq_r.at[d], dev(y=yi(d)))

    def stage_heads():
        for d in range(1, Y):
            there = pl.ds(pl.multiple_of(yi(-d) * (HEAD // Y), HEAD // Y), HEAD // Y)
            arrive(pbuf.at[there], pq_s.at[d], pq_r.at[d])
        prior = pbuf[...]
        for k in range(Y - 1):
            a_k = decay_of(ybuf[k, HEAD : HEAD + 16, :])
            prior = jnp.where(k < y, a_k * prior + ybuf[k, 0:HEAD, :].astype(F32), prior)
        recur = local_out[...] + lax.dot_general(
            q_decay[...], prior, NT, precision=EXACT, preferred_element_type=F32
        )
        ep = emit_pre[...].astype(F32)
        norm = lax.rsqrt(jnp.mean(recur * recur, axis=-1, keepdims=True) + EPS)
        mixed[...] = (recur * norm * head_gain[...] * (ep * sigmoid(ep))).astype(BF16)
        heads[:, cols(x, c)] = mixed[...]
        dst = heads.at[:, cols(x, c)]
        for d in range(1, X):
            send(mixed, dst, hx_s.at[d], hx_r.at[d], dev(x=xi(d)))
        send(mixed, dst, hc_s.at[0], hc_r.at[0], dev(c=1 - c))

    def cols(xk, ck):
        return pl.ds(pl.multiple_of((xk * C + ck) * HEAD, HEAD), HEAD)

    def stage_heads2():
        for d in range(1, X):
            ref = heads.at[:, cols(xi(-d), c)]
            arrive(ref, hx_s.at[d], hx_r.at[d])
            send(ref, ref, hc_s.at[d], hc_r.at[d], dev(c=1 - c))

    def stage_norm():
        for i in range(2):
            arrive(wo.at[orows(xi(2 * i - 1), 1 - c)], wc_s.at[1 + i], wc_r.at[1 + i])
            arrive(wo.at[orows(xi(2), 1 - c, 64, 64 * i)], wc_s.at[3 + i], wc_r.at[3 + i])
        arrive(wo.at[orows(x, 1 - c)], wc_s.at[0], wc_r.at[0])
        for d in range(0, X):
            arrive(heads.at[:, cols(xi(-d), 1 - c)], hc_s.at[d], hc_r.at[d])
        tile = 256

        def project(n, square):
            at = pl.ds(pl.multiple_of(n * tile, tile), tile)
            got = resid[:, at].astype(F32) + jnp.dot(
                heads[...], wo[:, at], preferred_element_type=F32
            )
            after[:, at] = got
            return square + jnp.sum(got * got, axis=-1, keepdims=True)

        square = lax.fori_loop(0, D // tile, project, jnp.zeros((ROWS, 1), F32))
        after_scale[...] = lax.rsqrt(square * (1.0 / D) + EPS)

        def scaled(n, carry):
            at = pl.ds(pl.multiple_of(n * tile, tile), tile)
            for j in range(2):
                half = pl.ds(pl.multiple_of(jnp.where(j == 0, 1 - c, c) * 128, 128), 128)
                normed[128 * j : 128 * (j + 1), at] = (
                    after[half, at] * after_scale[half, :] * norm_gain[:, at]
                ).astype(BF16)
            return carry

        lax.fori_loop(0, D // tile, scaled, 0)

    stages = {
        1: [stage_wout],
        2: [stage_z],
        3: [stage_heads, stage_wout2],
        4: [stage_heads2],
        5: [stage_norm],
    }

    pending = [(0, z)]
    ended = []
    for step in range(1, STEPS + 1):
        fresh = []
        for i in range(2):
            if i == 1 and step == STEPS:
                continue
            zk = zi((2 * i - 1) * step)
            for u in range(2):
                arrive(wb.at[u, rows32(zk, y)], b1_s.at[i, u, step], b1_r.at[i, u, step])
            if step + 1 <= STEPS - i:
                send_b(i, step + 1, zk)
            k = 2 * step - 1 + i
            send_y(k, zk)
            fresh.append((k, zk))
        for i in range(2):
            if i == 1 and step == STEPS:
                continue
            zk = zi((2 * i - 1) * step)
            for u in range(2):
                arrive(wa.at[u, group(zk)], a2_s.at[i, u, step], a2_r.at[i, u, step])
                if step + 1 <= STEPS - i:
                    ref = wa.at[u, group(zk)]
                    send(
                        ref,
                        ref,
                        a2_s.at[i, u, step + 1],
                        a2_r.at[i, u, step + 1],
                        dev(z=zi(1 - 2 * i)),
                    )
        for k, zk in pending:
            relay_y(k, zk)
        for k, zk in ended:
            end_y(k, zk)
        ended, pending = pending, fresh
        for stage in stages.get(step, []):
            stage()
    for k, zk in pending:
        relay_y(k, zk)
    for k, zk in ended + pending:
        end_y(k, zk)

    for buf, w, width in ((hid_a, wa, NA), (hid_b, wb, NB)):
        for at in range(0, width, 256):
            n = min(256, width - at)
            h = jnp.dot(normed[...], w[0, :, at : at + n], preferred_element_type=F32)
            h = jnp.maximum(h, 0.0)
            buf[:, at : at + n] = (h * h).astype(BF16)
    tile = 256
    per = HW // tile
    for h in range(HALVES):

        def contract(n, carry, h=h):
            fr = pl.ds(pl.multiple_of(h * HW + n * tile, tile), tile)
            at = pl.ds(pl.multiple_of(n * tile, tile), tile)
            got = lax.dot_general(hid_a[...], wa[1, fr, :], NT, preferred_element_type=F32)
            got += lax.dot_general(hid_b[...], wb[1, fr, :], NT, preferred_element_type=F32)
            pair_out[h, :, at] = got[0:128].astype(BF16)
            own_sum[h, :, at] = got[128:256]
            return carry

        lax.fori_loop(0, per, contract, 0)
        send(pair_out.at[h], pair_in.at[h], pp_s.at[h], pp_r.at[h], dev(c=1 - c))

    def blk(xk):
        return pl.ds(pl.multiple_of(xk * 32, 32), 32)

    for h in range(HALVES):
        arrive(pair_in.at[h], pp_s.at[h], pp_r.at[h])
        own_sum[h] = own_sum[h] + pair_in[h].astype(F32)
        for d in range(1, X):
            rs_out[h, d - 1] = own_sum[h, blk(xi(d)), :].astype(BF16)
            send(
                rs_out.at[h, d - 1],
                rs_in.at[h, d - 1],
                rs_s.at[h, d],
                rs_r.at[h, d],
                dev(x=xi(d)),
            )

    def orow(xk, ck):
        return pl.ds(pl.multiple_of(ck * 128 + xk * 32, 32), 32)

    for h in range(HALVES):
        hc = pl.ds(h * HW, HW)
        total = after[orow(x, c), hc] + own_sum[h, blk(x), :]
        for d in range(1, X):
            arrive(rs_in.at[h, d - 1], rs_s.at[h, d], rs_r.at[h, d])
            total = total + rs_in[h, d - 1].astype(F32)
        fin[h] = total.astype(BF16)
        out[orow(x, c), hc] = fin[h]
        dst = out.at[orow(x, c), hc]
        for d in range(1, X):
            send(fin.at[h], dst, gx_s.at[h, d], gx_r.at[h, d], dev(x=xi(d)))
        send(fin.at[h], dst, gc_s.at[h, 0], gc_r.at[h, 0], dev(c=1 - c))
    for h in range(HALVES):
        hc = pl.ds(h * HW, HW)
        for d in range(1, X):
            ref = out.at[orow(xi(-d), c), hc]
            arrive(ref, gx_s.at[h, d], gx_r.at[h, d])
            send(ref, ref, gc_s.at[h, d], gc_r.at[h, d], dev(c=1 - c))
    for h in range(HALVES):
        hc = pl.ds(h * HW, HW)
        for d in range(0, X):
            arrive(out.at[orow(xi(-d), 1 - c), hc], gc_s.at[h, d], gc_r.at[h, d])
    for cp in sent:
        cp.wait_send()
    for d in range(1, Z):

        @pl.when(z + d < Z)
        def _():
            rdma(zsend, zbuf.at[z], zs_s.at[d], zs_r.at[d], dev(z=zi(d))).wait_send()


def body(
    resid,
    read_pre,
    keep_pre,
    written,
    emit_pre,
    shrink,
    floor_c,
    head_gain,
    wout,
    norm_gain,
    up,
    down,
):
    vm = pl.BlockSpec(memory_space=pltpu.VMEM)
    hbm = pl.BlockSpec(memory_space=pltpu.HBM)
    dma = pltpu.SemaphoreType.DMA
    call = pl.pallas_call(
        kernel,
        out_shape=jax.ShapeDtypeStruct((ROWS, D), BF16),
        in_specs=[vm] * 8 + [hbm, vm, hbm, hbm],
        out_specs=vm,
        scratch_shapes=[
            pltpu.VMEM((2, D, NA), BF16),
            pltpu.VMEM((2, D, NB), BF16),
            pltpu.VMEM((MIX, D), BF16),
            pltpu.VMEM((ROWS, D), F32),
            pltpu.VMEM((ROWS, 1), F32),
            pltpu.VMEM((ROWS, D), BF16),
            pltpu.VMEM((ROWS, NA), BF16),
            pltpu.VMEM((ROWS, NB), BF16),
            pltpu.VMEM((ROWS, MIX), BF16),
            pltpu.VMEM((ROWS, HEAD), F32),
            pltpu.VMEM((ROWS, HEAD), F32),
            pltpu.VMEM((ROWS, HEAD), BF16),
            pltpu.VMEM((Y, HEAD + 16, HEAD), BF16),
            pltpu.VMEM((HEAD // Y + 16, HEAD), BF16),
            pltpu.VMEM((Z, HEAD // Y + 16, HEAD), BF16),
            pltpu.VMEM((HEAD, HEAD), F32),
            pltpu.VMEM((HALVES, 128, HW), BF16),
            pltpu.VMEM((HALVES, 128, HW), BF16),
            pltpu.VMEM((HALVES, 128, HW), F32),
            pltpu.VMEM((HALVES, X - 1, 32, HW), BF16),
            pltpu.VMEM((HALVES, X - 1, 32, HW), BF16),
            pltpu.VMEM((HALVES, 32, HW), BF16),
            dma((5,)),
            dma((2, Y)),
            dma((2, Y)),
            dma((2, 2, STEPS + 1)),
            dma((2, 2, STEPS + 1)),
            dma((2, 2, STEPS + 1)),
            dma((2, 2, STEPS + 1)),
            dma((2, 2, Z)),
            dma((2, 2, Z)),
            dma((2, 2, Z)),
            dma((2, 2, Z)),
            dma((Y,)),
            dma((Y,)),
            dma((Z,)),
            dma((Z,)),
            dma((Y,)),
            dma((Y,)),
            dma((4,)),
            dma((4,)),
            dma((5,)),
            dma((5,)),
            dma((X,)),
            dma((X,)),
            dma((X,)),
            dma((X,)),
            dma((HALVES,)),
            dma((HALVES,)),
            dma((HALVES, X)),
            dma((HALVES, X)),
            dma((HALVES, X)),
            dma((HALVES, X)),
            dma((HALVES, X)),
            dma((HALVES, X)),
        ],
        compiler_params=pltpu.CompilerParams(
            collective_id=0, has_side_effects=True, vmem_limit_bytes=60 * 1024 * 1024
        ),
        name="layer",
    )
    return call(
        resid,
        read_pre,
        keep_pre,
        written,
        emit_pre,
        shrink,
        floor_c.reshape(1, -1),
        head_gain.reshape(1, -1),
        wout,
        norm_gain.reshape(1, -1),
        up,
        down,
    )


def solution(mesh):
    finer = Mesh(mesh.devices.reshape(Z, Y, X, C), ("z", "y", "x", "c"))
    sp, tp = ("z", "y"), ("x", "c")
    return jax.shard_map(
        body,
        mesh=finer,
        in_specs=(
            P(sp, None),
            P(sp, tp),
            P(sp, tp),
            P(sp, tp),
            P(sp, tp),
            P(sp, tp),
            P(tp),
            P(),
            P(tp, None),
            P(),
            P(sp, tp),
            P(sp, tp),
        ),
        out_specs=P(sp, None),
        check_vma=False,
    )
```

time: 364 us -> 114 us (0.31)
  waiting for transfers between devices: 251 us -> 0 us
  Pallas kernels: 0 us -> 112 us
  blocking collectives: 53.4 us -> 0 us
  matrix products: 15.7 us -> 0 us
  other arithmetic: 14.3 us -> 0 us
  between operations: 13.4 us -> 0.01 us
  starting transfers between devices: 12.8 us -> 0 us
    all_gather x3 -> x0, waiting for transfers between devices: 235 us -> none  [the longest x1 147 us: in_one_piece(): whole = lax.all_gather(both, axis, axis=dim, tiled=True)]
    pallas_call x0 -> x1, Pallas kernels: none -> 112 us  [body(): call(resid, read_pre, keep_pre, written, emit_pre, shrink, floor_c.reshap...]
    all_to_all x2 -> x0, blocking collectives: 42.6 us -> none  [copy_for_each(): lax.all_to_all(jnp.broadcast_to(shard[None], (peers, *shard.shape)), axis...]
    dot_general x15 -> x0, matrix products: 15.7 us -> none  [the longest x1 6.83 us: body(): lax.dot_general(hidden, down_whole, (((1,), (1,)), ((), ())), preferred_e...]
    all_to_all x1 -> x0, waiting for transfers between devices: 15 us -> none  [sum_at_owner(): lax.all_to_all(blocks, axis, split_axis=0, concat_axis=0, tiled=True)]
    all_to_all x1 -> x0, starting transfers between devices: 12.7 us -> none  [sum_at_owner(): lax.all_to_all(blocks, axis, split_axis=0, concat_axis=0, tiled=True)]
    all_gather x1 -> x0, blocking collectives: 10.7 us -> none  [gathered_once(): both, at, found = (lax.all_gather(jnp.concatenate(lines), axis), 0, {})]
    dot_general x4 -> x0, other arithmetic: 6.81 us -> none  [block_step(): jnp.einsum('htk,hsk,htsk->hts', query_block_rows, key_blk, decay, precisi...]
  transfers between devices with their start and end apart: 4 -> 0, of which waited for: 4 -> 0; matrix products, arithmetic and copies ran while one was open for 2% -> 0% of each run, Pallas kernels for 0% -> 0%
where the time goes in v1:
time: 114 us
  Pallas kernels  112 us (98%)
  local copies, waits for them, and re-layouts  2.3 us (2%)
    pallas_call x1, Pallas kernels, body(): call(resid, read_pre, keep_pre, written, emit_pre, shrink, floor_c.reshap...  112 us
    unnamed x1, local copies, waits for them, and re-layouts  2.3 us

profile of v1, /device:TPU:1, one launch (start us, length us, event | category | flops | bytes accessed | tf_op | source)
XLA Modules:
  0.0 114.0 jit_solution(2879947339051844841)
XLA Ops:
  0.0 111.7 %layer.1 = bf16[256,2048]{1,0:T(8,128)(2,1)} custom-call(bf16[256,2048]{1,0:T(8,128)(2,1)} %resid.1, bf16[256,128]{1,0:T(8,128)(2,1)} %read_pre.1, bf16[256,128]{1,0:T(8,128)(2,1)} %keep_pre.1, bf16[256,128]{1,0:T(8,128)(2,1)} %written.1, bf16[256,128]{1,0:T(8,128)(2,1)} %emit_pre.1, f32[256,128]{1,0:T(8,128)} %shrink.1, f32[1,128]{1,0:T(1,128)} %bitcast.4, ...), custom_call_target="tpu_custom_call" | custom-call | tf_op jit(solution)/shard_map/layer/pallas_call | solution.py:610
  111.7 2.3 %copy.14 = bf16[256,2048]{1,0:T(8,128)(2,1)} copy(bf16[256,2048]{1,0:T(8,128)(2,1)} %layer.1) | data formatting | bytes 2097152

commit v2 on v1

v2 whole, which is shorter than its diff:
```python
import jax
import jax.numpy as jnp
from jax import lax
from jax.experimental import pallas as pl
from jax.experimental.pallas import tpu as pltpu
from jax.sharding import Mesh
from jax.sharding import PartitionSpec as P

Z, Y, X, C = 16, 4, 4, 2
HEAD = 128
BLOCK = 64
ROWS = 256
D = 2048
MIX = 1024
HID = 1024
NA = 384
NB = HID - NA
SP_N = Z * Y
WR = D // SP_N
G = 4
STEPS = Z // 2
LAG = 0
CUTS = ((10, 4), (12, 10), (13, 16))
NB_CUT = len(CUTS)
F32 = jnp.float32
BF16 = jnp.bfloat16
EPS = 1e-06
EXACT = lax.Precision.HIGHEST
NT = (((1,), (1,)), ((), ()))
TN = (((0,), (0,)), ((), ()))


def sigmoid(x):
    return 1.0 / (1.0 + jnp.exp(-x))


def log_one_minus(u):
    series = jnp.zeros_like(u)
    for k in range(9, 0, -1):
        series = u * (1.0 / k + series)
    return jnp.where(u < 0.125, -series, jnp.log(1.0 - u))


def one_minus_exp(w):
    series = jnp.ones_like(w)
    for k in range(10, 1, -1):
        series = 1.0 + (w * (1.0 / k)) * series
    return jnp.where(w > -0.5, -w * series, 1.0 - jnp.exp(w))


def kernel(
    resid_in,
    read_in,
    keep_in,
    written_in,
    emit_in,
    shrink_in,
    floor_in,
    head_gain_in,
    wout_in,
    norm_gain_in,
    up_in,
    down_in,
    out,
    wa,
    wb,
    wo,
    read_pre,
    keep_pre,
    written,
    emit_pre,
    shrink,
    floor_c,
    head_gain,
    norm_gain,
    resid,
    after,
    after_scale,
    normed,
    hid_a,
    hid_b,
    heads,
    local_out,
    q_decay,
    mixed,
    ybuf,
    zsend,
    zbuf,
    gsend,
    gbuf,
    pbuf,
    pair_out,
    pair_in,
    own_sum,
    rs_out,
    rs_in,
    ag,
    know,
    lsem,
    a1_s,
    a1_r,
    a2_s,
    a2_r,
    b1_s,
    b1_r,
    yf_s,
    yf_r,
    yh_s,
    yh_r,
    st_s,
    st_r,
    zs_s,
    zs_r,
    gs_s,
    gs_r,
    pq_s,
    pq_r,
    wx_s,
    wx_r,
    wc_s,
    wc_r,
    hx_s,
    hx_r,
    hc_s,
    hc_r,
    pp_s,
    pp_r,
    rs_s,
    rs_r,
    gx_s,
    gx_r,
    gc_s,
    gc_r,
):
    z = lax.axis_index("z")
    y = lax.axis_index("y")
    x = lax.axis_index("x")
    c = lax.axis_index("c")
    tp = x * C + c

    def zi(d):
        return lax.rem(z + (d + Z), Z)

    def yi(d):
        return lax.rem(y + (d + Y), Y)

    def xi(d):
        return lax.rem(x + (d + X), X)

    def dev(**kw):
        at = {"z": z, "y": y, "x": x, "c": c}
        at.update(kw)
        return (at["z"], at["y"], at["x"], at["c"])

    def rdma(src, dst, s, r, to):
        return pltpu.make_async_remote_copy(
            src_ref=src,
            dst_ref=dst,
            send_sem=s,
            recv_sem=r,
            device_id=to,
            device_id_type=pl.DeviceIdType.MESH,
        )

    sent = []

    def send(src, dst, s, r, to):
        cp = rdma(src, dst, s, r, to)
        cp.start()
        sent.append(cp)

    def arrive(ref, s, r):
        rdma(ref, ref, s, r, dev(c=1 - c)).wait_recv()

    bar = pltpu.get_barrier_semaphore()
    peers = [dev(z=zi(d)) for d in (1, Z - 1)]
    peers += [dev(y=yi(d)) for d in range(1, Y)]
    peers += [dev(x=xi(d)) for d in range(1, X)]
    peers += [dev(c=1 - c)]
    for p in peers:
        pl.semaphore_signal(bar, inc=1, device_id=p, device_id_type=pl.DeviceIdType.MESH)

    def rows32(zk, yk, n=WR, off=0):
        return pl.ds(pl.multiple_of((zk * Y + yk) * WR + off, 16), n)

    def a_own():
        return rows32(z, y)

    local = []
    for u, src in ((0, up_in), (1, down_in)):
        local.append(
            pltpu.make_async_copy(src.at[:, pl.ds(0, NA)], wa.at[u, a_own()], lsem.at[2 * u])
        )
        local.append(
            pltpu.make_async_copy(src.at[:, pl.ds(NA, NB)], wb.at[u, a_own()], lsem.at[2 * u + 1])
        )

    def orows(xk, ck, n=HEAD, off=0):
        return pl.ds(pl.multiple_of((xk * C + ck) * HEAD + off, 64), n)

    local.append(pltpu.make_async_copy(wout_in, wo.at[orows(x, c)], lsem.at[4]))
    for cp in local:
        cp.start()
    small = []
    for src, dst in (
        (floor_in, floor_c),
        (keep_in, keep_pre),
        (shrink_in, shrink),
        (read_in, read_pre),
        (written_in, written),
        (emit_in, emit_pre),
        (head_gain_in, head_gain),
        (norm_gain_in, norm_gain),
    ):
        small.append(pltpu.make_async_copy(src, dst, lsem.at[6 + len(small)]))
    for cp in small:
        cp.start()
    resid_copy = pltpu.make_async_copy(resid_in, resid, lsem.at[5])
    resid_copy.start()

    for cp in local:
        cp.wait()
    pl.semaphore_wait(bar, len(peers))

    def tell(n):
        for d in (1 << n, Z - (1 << n)):
            pl.semaphore_signal(
                know.at[n], inc=1, device_id=dev(z=zi(d)), device_id_type=pl.DeviceIdType.MESH
            )

    tell(0)
    def send_b(u, i, step, zk):
        ref = wb.at[u, rows32(zk, y)]
        send(ref, ref, b1_s.at[i, u, step], b1_r.at[i, u, step], dev(z=zi(1 - 2 * i)))

    def send_y(u, k, zk):
        ref = wb.at[u, rows32(zk, y)]
        for i in range(2):
            send(ref, ref, yf_s.at[i, u, k], yf_r.at[i, u, k], dev(y=yi(1 - 2 * i)))

    def relay_y(u, k, zk):
        for i in range(2):
            yk = yi(2 * i - 1)
            arrive(wb.at[u, rows32(zk, yk)], yf_s.at[i, u, k], yf_r.at[i, u, k])
            ref = wb.at[u, rows32(zk, yk, 16, 16 * i)]
            send(ref, ref, yh_s.at[i, u, k], yh_r.at[i, u, k], dev(y=yi(1 - 2 * i)))

    def end_y(u, k, zk):
        for i in range(2):
            ref = wb.at[u, rows32(zk, yi(2), 16, 16 * i)]
            arrive(ref, yh_s.at[i, u, k], yh_r.at[i, u, k])

    def group(zk):
        return pl.ds(pl.multiple_of(zk * (Y * WR), Y * WR), Y * WR)

    def send_a(u, i, step, zk, j):
        ref = wa.at[u, group(zk)]
        send(ref, ref, a2_s.at[i, u, step, j], a2_r.at[i, u, step, j], dev(z=zi(1 - 2 * i)))

    for i in range(2):
        send_b(0, i, 1, z)
    for u in range(2):
        for d in range(1, Y):
            ref = wa.at[u, a_own()]
            send(ref, ref, a1_s.at[u, d], a1_r.at[u, d], dev(y=yi(d)))
    for u in range(2):
        send_y(u, 0, z)
    own_wo = wo.at[orows(x, c)]
    for i in range(2):
        send(own_wo, own_wo, wx_s.at[i], wx_r.at[i], dev(x=xi(1 - 2 * i)))
    send(own_wo, own_wo, wc_s.at[0], wc_r.at[0], dev(c=1 - c))

    for cp in small:
        cp.wait()
    floor = floor_c[...]
    pre = keep_pre[...].astype(F32)
    logs = log_one_minus(floor * (1.0 / (1.0 + jnp.exp(pre)))) + shrink[...]
    key = one_minus_exp(logs)
    rp = read_pre[...].astype(F32)
    query = rp * sigmoid(rp)
    value = written[...].astype(F32)
    ti = lax.broadcasted_iota(jnp.int32, (BLOCK, BLOCK), 0)
    si = lax.broadcasted_iota(jnp.int32, (BLOCK, BLOCK), 1)
    lower = ti >= si
    tri = lower.astype(F32)
    state = jnp.zeros((HEAD, HEAD), F32)
    base = jnp.zeros((1, HEAD), F32)
    parts = []
    for k in range(ROWS // BLOCK):
        sl = slice(k * BLOCK, (k + 1) * BLOCK)
        lc = jnp.dot(tri, logs[sl], precision=EXACT, preferred_element_type=F32)
        end = lc[BLOCK - 1 :, :]
        kd = key[sl] * jnp.exp(end - lc)
        parts.append((sl, lc, state))
        q_decay[sl, :] = query[sl] * jnp.exp(lc + base)
        state = jnp.exp(end) * state + lax.dot_general(
            value[sl], kd, TN, precision=EXACT, preferred_element_type=F32
        )
        base = base + end
    decay = jnp.exp(base)

    def two_parts(a):
        hi = a.astype(BF16)
        lo = (a - hi.astype(F32)).astype(BF16)
        r = lax.broadcasted_iota(jnp.int32, (16, HEAD), 0)
        both = jnp.where(r == 0, hi.astype(F32), jnp.where(r == 1, lo.astype(F32), 0.0))
        return both.astype(BF16)

    ybuf[y, 0:HEAD, :] = state.astype(BF16)
    ybuf[y, HEAD : HEAD + 16, :] = two_parts(decay)

    for d in range(1, Y):
        send(ybuf.at[y], ybuf.at[y], st_s.at[d], st_r.at[d], dev(y=yi(d)))

    for sl, lc, st in parts:
        qd = query[sl] * jnp.exp(lc)
        kd = key[sl] * jnp.exp(-lc)
        scores = lax.dot_general(qd, kd, NT, precision=EXACT, preferred_element_type=F32)
        scores = jnp.where(lower, scores, 0.0)
        local_out[sl, :] = jnp.dot(
            scores, value[sl], precision=EXACT, preferred_element_type=F32
        ) + lax.dot_general(qd, st, NT, precision=EXACT, preferred_element_type=F32)

    pl.semaphore_wait(know.at[0], 2)
    tell(1)
    for u in range(2):
        for d in range(1, Y):
            arrive(wa.at[u, rows32(z, yi(-d))], a1_s.at[u, d], a1_r.at[u, d])
        if u == 0:
            for i in range(2):
                send_a(0, i, 1, z, 0)
    for i in range(2):
        send_b(1, i, 1, z)
    for i in range(2):
        send_a(1, i, 1, z, 0)

    def decay_of(block):
        return block[0:1, :].astype(F32) + block[1:2, :].astype(F32)

    for d in range(1, Y):
        arrive(ybuf.at[yi(-d)], st_s.at[d], st_r.at[d])
    quarter = pl.ds(pl.multiple_of(y * (HEAD // Y), HEAD // Y), HEAD // Y)
    row_q = jnp.zeros((HEAD // Y, HEAD), F32)
    row_a = jnp.ones((1, HEAD), F32)
    for k in range(Y):
        a_k = decay_of(ybuf[k, HEAD : HEAD + 16, :])
        row_q = a_k * row_q + ybuf[k, quarter, :].astype(F32)
        row_a = row_a * a_k
    zsend[0 : HEAD // Y, :] = row_q.astype(BF16)
    zsend[HEAD // Y : HEAD // Y + 16, :] = two_parts(row_a)

    grp = z // G
    inner = z % G

    def zg(d):
        return grp * G + lax.rem(inner + (d + G), G)

    def stage_zsend():
        pl.semaphore_wait(know.at[1], 2)
        tell(2)
        for d in range(1, G):
            send(zsend, zbuf.at[inner], zs_s.at[d], zs_r.at[d], dev(z=zg(d)))

    def decay_rows(ref, k):
        return decay_of(ref[k, HEAD // Y : HEAD // Y + 16, :])

    def stage_zgroup():
        for d in range(1, G):
            arrive(zbuf.at[lax.rem(inner + (G - d), G)], zs_s.at[d], zs_r.at[d])
        zbuf[inner] = zsend[...]
        pl.semaphore_wait(know.at[2], 2)
        total = jnp.zeros((HEAD // Y, HEAD), F32)
        total_a = jnp.ones((1, HEAD), F32)
        for k in range(G):
            a_k = decay_rows(zbuf, k)
            total = a_k * total + zbuf[k, 0 : HEAD // Y, :].astype(F32)
            total_a = total_a * a_k
        gsend[0 : HEAD // Y, :] = total.astype(BF16)
        gsend[HEAD // Y : HEAD // Y + 16, :] = two_parts(total_a)
        for d in range(1, Z // G):

            @pl.when(grp + d < Z // G)
            def _():
                rdma(gsend, gbuf.at[grp], gs_s.at[d], gs_r.at[d], dev(z=zi(d * G))).start()

    def stage_wout():
        for i in range(2):
            xk = xi(2 * i - 1)
            full = wo.at[orows(xk, c)]
            arrive(full, wx_s.at[i], wx_r.at[i])
            half = wo.at[orows(xk, c, 64, 64 * i)]
            send(half, half, wx_s.at[2 + i], wx_r.at[2 + i], dev(x=xi(1 - 2 * i)))
            send(full, full, wc_s.at[1 + i], wc_r.at[1 + i], dev(c=1 - c))

    def stage_wout2():
        for i in range(2):
            half = wo.at[orows(xi(2), c, 64, 64 * i)]
            arrive(half, wx_s.at[2 + i], wx_r.at[2 + i])
            send(half, half, wc_s.at[3 + i], wc_r.at[3 + i], dev(c=1 - c))

    def stage_z():
        for d in range(1, Z // G):

            @pl.when(grp - d >= 0)
            def _():
                arrive(gbuf.at[grp - d], gs_s.at[d], gs_r.at[d])

        def add(k, acc):
            return decay_rows(gbuf, k) * acc + gbuf[k, 0 : HEAD // Y, :].astype(F32)

        def add_in(k, acc):
            return decay_rows(zbuf, k) * acc + zbuf[k, 0 : HEAD // Y, :].astype(F32)

        before = lax.fori_loop(0, grp, add, jnp.zeros((HEAD // Y, HEAD), F32))
        pbuf[quarter, :] = lax.fori_loop(0, inner, add_in, before)
        for d in range(1, Y):
            ref = pbuf.at[quarter]
            send(ref, ref, pq_s.at[d], pq_r.at[d], dev(y=yi(d)))

    def stage_heads():
        for d in range(1, Y):
            there = pl.ds(pl.multiple_of(yi(-d) * (HEAD // Y), HEAD // Y), HEAD // Y)
            arrive(pbuf.at[there], pq_s.at[d], pq_r.at[d])
        prior = pbuf[...]
        for k in range(Y - 1):
            a_k = decay_of(ybuf[k, HEAD : HEAD + 16, :])
            prior = jnp.where(k < y, a_k * prior + ybuf[k, 0:HEAD, :].astype(F32), prior)
        recur = local_out[...] + lax.dot_general(
            q_decay[...], prior, NT, precision=EXACT, preferred_element_type=F32
        )
        ep = emit_pre[...].astype(F32)
        norm = lax.rsqrt(jnp.mean(recur * recur, axis=-1, keepdims=True) + EPS)
        mixed[...] = (recur * norm * head_gain[...] * (ep * sigmoid(ep))).astype(BF16)
        heads[:, cols(x, c)] = mixed[...]
        dst = heads.at[:, cols(x, c)]
        for d in range(1, X):
            send(mixed, dst, hx_s.at[d], hx_r.at[d], dev(x=xi(d)))
        send(mixed, dst, hc_s.at[0], hc_r.at[0], dev(c=1 - c))

    def cols(xk, ck):
        return pl.ds(pl.multiple_of((xk * C + ck) * HEAD, HEAD), HEAD)

    def stage_heads2():
        for d in range(1, X):
            ref = heads.at[:, cols(xi(-d), c)]
            arrive(ref, hx_s.at[d], hx_r.at[d])
            send(ref, ref, hc_s.at[d], hc_r.at[d], dev(c=1 - c))

    tile = 256

    def stage_gathered():
        for i in range(2):
            arrive(wo.at[orows(xi(2 * i - 1), 1 - c)], wc_s.at[1 + i], wc_r.at[1 + i])
            arrive(wo.at[orows(xi(2), 1 - c, 64, 64 * i)], wc_s.at[3 + i], wc_r.at[3 + i])
        arrive(wo.at[orows(x, 1 - c)], wc_s.at[0], wc_r.at[0])
        for d in range(0, X):
            arrive(heads.at[:, cols(xi(-d), 1 - c)], hc_s.at[d], hc_r.at[d])
        resid_copy.wait()
        after_scale[...] = jnp.zeros((ROWS, 1), F32)

    def stage_project(lo, hi):
        def project(n, square):
            at = pl.ds(pl.multiple_of(n * tile, tile), tile)
            got = resid[:, at].astype(F32) + jnp.dot(
                heads[...], wo[:, at], preferred_element_type=F32
            )
            after[:, at] = got
            return square + jnp.sum(got * got, axis=-1, keepdims=True)

        after_scale[...] = lax.fori_loop(lo, hi, project, after_scale[...])

    def stage_norm():
        after_scale[...] = lax.rsqrt(after_scale[...] * (1.0 / D) + EPS)

        def scaled(n, carry):
            at = pl.ds(pl.multiple_of(n * tile, tile), tile)
            for j in range(2):
                half = pl.ds(pl.multiple_of(jnp.where(j == 0, 1 - c, c) * 128, 128), 128)
                normed[128 * j : 128 * (j + 1), at] = (
                    after[half, at] * after_scale[half, :] * norm_gain[:, at]
                ).astype(BF16)
            return carry

        lax.fori_loop(0, D // tile, scaled, 0)

    def stage_up():
        for buf, w, width in ((hid_a, wa, NA), (hid_b, wb, NB)):
            for at in range(0, width, 256):
                n = min(256, width - at)
                h = jnp.dot(normed[...], w[0, :, at : at + n], preferred_element_type=F32)
                h = jnp.maximum(h, 0.0)
                buf[:, at : at + n] = (h * h).astype(BF16)

    def zk_of(k):
        return zi(k // 2 if k % 2 == 0 else -(k + 1) // 2)

    def blk(xk):
        return pl.ds(pl.multiple_of(xk * 32, 32), 32)

    def feat(k):
        return pl.ds(pl.multiple_of(zk_of(k) * 128, 128), 128)

    cuts = [(0 if b == 0 else CUTS[b - 1][1], CUTS[b][1]) for b in range(NB_CUT)]

    def down(b):
        lo, hi = cuts[b]
        for k in range(lo, hi):
            fr = feat(k)
            got = lax.dot_general(hid_a[...], wa[1, fr, :], NT, preferred_element_type=F32)
            got += lax.dot_general(hid_b[...], wb[1, fr, :], NT, preferred_element_type=F32)
            pair_out[k] = got[0:128].astype(BF16)
            own_sum[k] = got[128:256]
        part = pl.ds(lo, hi - lo)
        send(pair_out.at[part], pair_in.at[part], pp_s.at[b], pp_r.at[b], dev(c=1 - c))

    def scatter(b):
        lo, hi = cuts[b]
        part = pl.ds(lo, hi - lo)
        arrive(pair_in.at[part], pp_s.at[b], pp_r.at[b])
        own_sum[lo:hi] = own_sum[lo:hi] + pair_in[lo:hi].astype(F32)
        for d in range(1, X):
            rs_out[d - 1, lo:hi] = own_sum[lo:hi, blk(xi(d)), :].astype(BF16)
            src, dst = rs_out.at[d - 1, part], rs_in.at[d - 1, part]
            send(src, dst, rs_s.at[b, d], rs_r.at[b, d], dev(x=xi(d)))

    own_rows = pl.ds(pl.multiple_of(c * 128 + x * 32, 32), 32)

    def finish(b):
        lo, hi = cuts[b]
        part = pl.ds(lo, hi - lo)
        for d in range(1, X):
            arrive(rs_in.at[d - 1, part], rs_s.at[b, d], rs_r.at[b, d])
        for k in range(lo, hi):
            total = after[own_rows, feat(k)] + own_sum[k, blk(x), :]
            for d in range(1, X):
                total = total + rs_in[d - 1, k].astype(F32)
            ag[c, x, k] = total.astype(BF16)
        ref = ag.at[c, x, part]
        for d in range(1, X):
            send(ref, ref, gx_s.at[b, d], gx_r.at[b, d], dev(x=xi(d)))
        send(ref, ref, gc_s.at[b, 0], gc_r.at[b, 0], dev(c=1 - c))

    def collect(b):
        lo, hi = cuts[b]
        part = pl.ds(lo, hi - lo)
        for d in range(1, X):
            ref = ag.at[c, xi(-d), part]
            arrive(ref, gx_s.at[b, d], gx_r.at[b, d])
            send(ref, ref, gc_s.at[b, d], gc_r.at[b, d], dev(c=1 - c))

    def unpack(b):
        lo, hi = cuts[b]
        part = pl.ds(lo, hi - lo)
        for d in range(0, X):
            arrive(ag.at[1 - c, xi(-d), part], gc_s.at[b, d], gc_r.at[b, d])
        for k in range(lo, hi):
            for ck in range(C):
                for xk in range(X):
                    r = ck * 128 + xk * 32
                    out[r : r + 32, feat(k)] = ag[ck, xk, k]

    def call(f, *a):
        return lambda: f(*a)

    stages = {
        0: [stage_zsend],
        2: [stage_zgroup],
        4: [stage_z],
        5: [stage_heads, stage_wout],
        6: [stage_heads2],
        7: [stage_wout2, stage_gathered, call(stage_project, 0, 4)],
        8: [call(stage_project, 4, 8), stage_norm],
        9: [stage_up, call(down, 0), call(down, 1), call(scatter, 0)],
    }

    pending = {0: [(0, z)], 1: [(0, z)]}
    ended = {0: [], 1: []}
    marks = [0]
    for t in range(0, STEPS + LAG + 2):
        for u, s in ((0, t), (1, t - LAG)):
            fresh = []
            for i in range(2):
                if 1 <= s + 1 <= STEPS - i:
                    step = s + 1
                    zk = zi((2 * i - 1) * step)
                    ref = wb.at[u, rows32(zk, y)]
                    arrive(ref, b1_s.at[i, u, step], b1_r.at[i, u, step])
                    if step + 1 <= STEPS - i:
                        send_b(u, i, step + 1, zk)
                    k = 2 * step - 1 + i
                    send_y(u, k, zk)
                    fresh.append((k, zk))
            for j in range(1):
                for i in range(2):
                    if 1 <= s <= STEPS - i:
                        zk = zi((2 * i - 1) * s)
                        ref = wa.at[u, group(zk)]
                        arrive(ref, a2_s.at[i, u, s, j], a2_r.at[i, u, s, j])
                        if s + 1 <= STEPS - i:
                            send_a(u, i, s + 1, zk, j)
            for k, zk in pending[u]:
                relay_y(u, k, zk)
            for k, zk in ended[u]:
                end_y(u, k, zk)
            ended[u], pending[u] = pending[u], fresh
        for stage in stages.get(t, []):
            stage()
        marks.append(len(sent))
        if len(marks) > 2:
            lo, hi = marks[-3], marks[-2]
            for cp in sent[lo:hi]:
                cp.wait_send()
    down(2)
    scatter(1)
    finish(0)
    scatter(2)
    finish(1)
    collect(0)
    finish(2)
    collect(1)
    unpack(0)
    collect(2)
    unpack(1)
    unpack(2)
    for cp in sent[marks[-2] :]:
        cp.wait_send()
    for d in range(1, Z // G):

        @pl.when(grp + d < Z // G)
        def _():
            rdma(gsend, gbuf.at[grp], gs_s.at[d], gs_r.at[d], dev(z=zi(d * G))).wait_send()


def body(
    resid,
    read_pre,
    keep_pre,
    written,
    emit_pre,
    shrink,
    floor_c,
    head_gain,
    wout,
    norm_gain,
    up,
    down,
):
    vm = pl.BlockSpec(memory_space=pltpu.VMEM)
    hbm = pl.BlockSpec(memory_space=pltpu.HBM)
    dma = pltpu.SemaphoreType.DMA
    call = pl.pallas_call(
        kernel,
        out_shape=jax.ShapeDtypeStruct((ROWS, D), BF16),
        in_specs=[hbm] * 12,
        out_specs=vm,
        scratch_shapes=[
            pltpu.VMEM((2, D, NA), BF16),
            pltpu.VMEM((2, D, NB), BF16),
            pltpu.VMEM((MIX, D), BF16),
            pltpu.VMEM((ROWS, HEAD), BF16),
            pltpu.VMEM((ROWS, HEAD), BF16),
            pltpu.VMEM((ROWS, HEAD), BF16),
            pltpu.VMEM((ROWS, HEAD), BF16),
            pltpu.VMEM((ROWS, HEAD), F32),
            pltpu.VMEM((1, HEAD), F32),
            pltpu.VMEM((1, HEAD), F32),
            pltpu.VMEM((1, D), F32),
            pltpu.VMEM((ROWS, D), BF16),
            pltpu.VMEM((ROWS, D), F32),
            pltpu.VMEM((ROWS, 1), F32),
            pltpu.VMEM((ROWS, D), BF16),
            pltpu.VMEM((ROWS, NA), BF16),
            pltpu.VMEM((ROWS, NB), BF16),
            pltpu.VMEM((ROWS, MIX), BF16),
            pltpu.VMEM((ROWS, HEAD), F32),
            pltpu.VMEM((ROWS, HEAD), F32),
            pltpu.VMEM((ROWS, HEAD), BF16),
            pltpu.VMEM((Y, HEAD + 16, HEAD), BF16),
            pltpu.VMEM((HEAD // Y + 16, HEAD), BF16),
            pltpu.VMEM((G, HEAD // Y + 16, HEAD), BF16),
            pltpu.VMEM((HEAD // Y + 16, HEAD), BF16),
            pltpu.VMEM((Z // G, HEAD // Y + 16, HEAD), BF16),
            pltpu.VMEM((HEAD, HEAD), F32),
            pltpu.VMEM((Z, 128, HEAD), BF16),
            pltpu.VMEM((Z, 128, HEAD), BF16),
            pltpu.VMEM((Z, 128, HEAD), F32),
            pltpu.VMEM((X - 1, Z, 32, HEAD), BF16),
            pltpu.VMEM((X - 1, Z, 32, HEAD), BF16),
            pltpu.VMEM((C, X, Z, 32, HEAD), BF16),
            pltpu.SemaphoreType.REGULAR((3,)),
            dma((14,)),
            dma((2, Y)),
            dma((2, Y)),
            dma((2, 2, STEPS + 1, Y)),
            dma((2, 2, STEPS + 1, Y)),
            dma((2, 2, STEPS + 1)),
            dma((2, 2, STEPS + 1)),
            dma((2, 2, Z)),
            dma((2, 2, Z)),
            dma((2, 2, Z)),
            dma((2, 2, Z)),
            dma((Y,)),
            dma((Y,)),
            dma((G,)),
            dma((G,)),
            dma((Z // G,)),
            dma((Z // G,)),
            dma((Y,)),
            dma((Y,)),
            dma((4,)),
            dma((4,)),
            dma((5,)),
            dma((5,)),
            dma((X,)),
            dma((X,)),
            dma((X,)),
            dma((X,)),
            dma((NB_CUT,)),
            dma((NB_CUT,)),
            dma((NB_CUT, X)),
            dma((NB_CUT, X)),
            dma((NB_CUT, X)),
            dma((NB_CUT, X)),
            dma((NB_CUT, X)),
            dma((NB_CUT, X)),
        ],
        compiler_params=pltpu.CompilerParams(
            collective_id=0, has_side_effects=True, vmem_limit_bytes=60 * 1024 * 1024
        ),
        name="layer",
    )
    return call(
        resid,
        read_pre,
        keep_pre,
        written,
        emit_pre,
        shrink,
        floor_c.reshape(1, -1),
        head_gain.reshape(1, -1),
        wout,
        norm_gain.reshape(1, -1),
        up,
        down,
    )


def solution(mesh):
    finer = Mesh(mesh.devices.reshape(Z, Y, X, C), ("z", "y", "x", "c"))
    sp, tp = ("z", "y"), ("x", "c")
    return jax.shard_map(
        body,
        mesh=finer,
        in_specs=(
            P(sp, None),
            P(sp, tp),
            P(sp, tp),
            P(sp, tp),
            P(sp, tp),
            P(sp, tp),
            P(tp),
            P(),
            P(tp, None),
            P(),
            P(sp, tp),
            P(sp, tp),
        ),
        out_specs=P(sp, None),
        check_vma=False,
    )
```

time: 114 us -> 102 us (0.89)
  Pallas kernels: 112 us -> 99.5 us
    pallas_call x1, Pallas kernels: 112 us -> 99.5 us  [body(): call(resid, read_pre, keep_pre, written, emit_pre, shrink, floor_c.reshap...]
where the time goes in v2:
time: 102 us
  Pallas kernels  99.5 us (98%)
  local copies, waits for them, and re-layouts  2.3 us (2%)
    pallas_call x1, Pallas kernels, body(): call(resid, read_pre, keep_pre, written, emit_pre, shrink, floor_c.reshap...  99.5 us
    unnamed x1, local copies, waits for them, and re-layouts  2.3 us

profile of v2, /device:TPU:1, one launch (start us, length us, event | category | flops | bytes accessed | tf_op | source)
XLA Modules:
  0.0 101.8 jit_solution(13204515345464187521)
XLA Ops:
  0.0 99.5 %layer.1 = bf16[256,2048]{1,0:T(8,128)(2,1)} custom-call(bf16[256,2048]{1,0:T(8,128)(2,1)} %resid_in.1, bf16[256,128]{1,0:T(8,128)(2,1)} %read_in.1, bf16[256,128]{1,0:T(8,128)(2,1)} %keep_in.1, bf16[256,128]{1,0:T(8,128)(2,1)} %written_in.1, bf16[256,128]{1,0:T(8,128)(2,1)} %emit_in.1, f32[256,128]{1,0:T(8,128)} %shrink_in.1, f32[1,128]{1,0:T(1,128)} %bitcast.4, ...), custom_call_target="tpu_custom_call" | custom-call | tf_op jit(solution)/shard_map/layer/pallas_call | solution.py:732
  99.5 2.3 %copy.14 = bf16[256,2048]{1,0:T(8,128)(2,1)} copy(bf16[256,2048]{1,0:T(8,128)(2,1)} %layer.1) | data formatting | bytes 2097152

commit v3 on v2

--- a/solution.py
+++ b/solution.py
@@ -20,7 +20,7 @@
 G = 4
 STEPS = Z // 2
 LAG = 0
-CUTS = ((10, 4), (12, 10), (13, 16))
+CUTS = (512, 1280, 2048)
 NB_CUT = len(CUTS)
 F32 = jnp.float32
 BF16 = jnp.bfloat16
@@ -94,7 +94,7 @@
     own_sum,
     rs_out,
     rs_in,
-    ag,
+    acc,
     know,
     lsem,
     a1_s,
@@ -483,94 +483,100 @@
 
         lax.fori_loop(0, D // tile, scaled, 0)
 
-    def stage_up():
-        for buf, w, width in ((hid_a, wa, NA), (hid_b, wb, NB)):
-            for at in range(0, width, 256):
-                n = min(256, width - at)
-                h = jnp.dot(normed[...], w[0, :, at : at + n], preferred_element_type=F32)
-                h = jnp.maximum(h, 0.0)
-                buf[:, at : at + n] = (h * h).astype(BF16)
-
     def zk_of(k):
         return zi(k // 2 if k % 2 == 0 else -(k + 1) // 2)
 
+    tiles = [(buf, w, at, min(256, n - at)) for buf, w, n in ((hid_a, wa, NA), (hid_b, wb, NB))
+             for at in range(0, n, 256)]
+
+    def partial_up(w, at, n, ks):
+        total = jnp.zeros((ROWS, n), F32)
+        for k in ks:
+            fr = group(zk_of(k))
+            total += jnp.dot(normed[:, fr], w[0, fr, at : at + n], preferred_element_type=F32)
+        return total
+
+    def stage_up_most():
+        for q, (_, w, at, n) in enumerate(tiles):
+            acc[q, :, 0:n] = partial_up(w, at, n, range(Z - 1))
+
+    def stage_up():
+        for q, (buf, w, at, n) in enumerate(tiles):
+            h = acc[q, :, 0:n] + partial_up(w, at, n, [Z - 1])
+            h = jnp.maximum(h, 0.0)
+            buf[:, at : at + n] = (h * h).astype(BF16)
+
     def blk(xk):
         return pl.ds(pl.multiple_of(xk * 32, 32), 32)
 
-    def feat(k):
-        return pl.ds(pl.multiple_of(zk_of(k) * 128, 128), 128)
-
-    cuts = [(0 if b == 0 else CUTS[b - 1][1], CUTS[b][1]) for b in range(NB_CUT)]
+    def orow(xk, ck):
+        return pl.ds(pl.multiple_of(ck * 128 + xk * 32, 32), 32)
+
+    own_rows = orow(x, c)
+    spans = [(0 if b == 0 else CUTS[b - 1], CUTS[b]) for b in range(NB_CUT)]
 
     def down(b):
-        lo, hi = cuts[b]
-        for k in range(lo, hi):
-            fr = feat(k)
-            got = lax.dot_general(hid_a[...], wa[1, fr, :], NT, preferred_element_type=F32)
-            got += lax.dot_general(hid_b[...], wb[1, fr, :], NT, preferred_element_type=F32)
-            pair_out[k] = got[0:128].astype(BF16)
-            own_sum[k] = got[128:256]
+        lo, hi = spans[b]
+        for f in range(lo, hi, 256):
+            at = slice(f, f + 256)
+            got = lax.dot_general(hid_a[...], wa[1, at, :], NT, preferred_element_type=F32)
+            got += lax.dot_general(hid_b[...], wb[1, at, :], NT, preferred_element_type=F32)
+            pair_out[:, at] = got[0:128].astype(BF16)
+            own_sum[:, at] = got[128:256]
         part = pl.ds(lo, hi - lo)
-        send(pair_out.at[part], pair_in.at[part], pp_s.at[b], pp_r.at[b], dev(c=1 - c))
+        send(pair_out.at[:, part], pair_in.at[:, part], pp_s.at[b], pp_r.at[b], dev(c=1 - c))
 
     def scatter(b):
-        lo, hi = cuts[b]
+        lo, hi = spans[b]
         part = pl.ds(lo, hi - lo)
-        arrive(pair_in.at[part], pp_s.at[b], pp_r.at[b])
-        own_sum[lo:hi] = own_sum[lo:hi] + pair_in[lo:hi].astype(F32)
-        for d in range(1, X):
-            rs_out[d - 1, lo:hi] = own_sum[lo:hi, blk(xi(d)), :].astype(BF16)
-            src, dst = rs_out.at[d - 1, part], rs_in.at[d - 1, part]
+        arrive(pair_in.at[:, part], pp_s.at[b], pp_r.at[b])
+        own_sum[:, lo:hi] = own_sum[:, lo:hi] + pair_in[:, lo:hi].astype(F32)
+        for d in (2, 1, 3):
+            rs_out[d - 1, :, lo:hi] = own_sum[blk(xi(d)), lo:hi].astype(BF16)
+            src, dst = rs_out.at[d - 1, :, part], rs_in.at[d - 1, :, part]
             send(src, dst, rs_s.at[b, d], rs_r.at[b, d], dev(x=xi(d)))
 
-    own_rows = pl.ds(pl.multiple_of(c * 128 + x * 32, 32), 32)
-
     def finish(b):
-        lo, hi = cuts[b]
+        lo, hi = spans[b]
         part = pl.ds(lo, hi - lo)
         for d in range(1, X):
-            arrive(rs_in.at[d - 1, part], rs_s.at[b, d], rs_r.at[b, d])
-        for k in range(lo, hi):
-            total = after[own_rows, feat(k)] + own_sum[k, blk(x), :]
-            for d in range(1, X):
-                total = total + rs_in[d - 1, k].astype(F32)
-            ag[c, x, k] = total.astype(BF16)
-        ref = ag.at[c, x, part]
+            arrive(rs_in.at[d - 1, :, part], rs_s.at[b, d], rs_r.at[b, d])
+        total = after[own_rows, lo:hi] + own_sum[blk(x), lo:hi]
         for d in range(1, X):
+            total = total + rs_in[d - 1, :, lo:hi].astype(F32)
+        out[own_rows, lo:hi] = total.astype(BF16)
+        ref = out.at[own_rows, part]
+        for d in (2, 1, 3):
             send(ref, ref, gx_s.at[b, d], gx_r.at[b, d], dev(x=xi(d)))
         send(ref, ref, gc_s.at[b, 0], gc_r.at[b, 0], dev(c=1 - c))
 
     def collect(b):
-        lo, hi = cuts[b]
+        lo, hi = spans[b]
         part = pl.ds(lo, hi - lo)
-        for d in range(1, X):
-            ref = ag.at[c, xi(-d), part]
+        for d in (1, 3, 2):
+            ref = out.at[orow(xi(-d), c), part]
             arrive(ref, gx_s.at[b, d], gx_r.at[b, d])
             send(ref, ref, gc_s.at[b, d], gc_r.at[b, d], dev(c=1 - c))
 
-    def unpack(b):
-        lo, hi = cuts[b]
+    def ended_batch(b):
+        lo, hi = spans[b]
         part = pl.ds(lo, hi - lo)
         for d in range(0, X):
-            arrive(ag.at[1 - c, xi(-d), part], gc_s.at[b, d], gc_r.at[b, d])
-        for k in range(lo, hi):
-            for ck in range(C):
-                for xk in range(X):
-                    r = ck * 128 + xk * 32
-                    out[r : r + 32, feat(k)] = ag[ck, xk, k]
+            arrive(out.at[orow(xi(-d), 1 - c), part], gc_s.at[b, d], gc_r.at[b, d])
 
     def call(f, *a):
         return lambda: f(*a)
 
     stages = {
         0: [stage_zsend],
-        2: [stage_zgroup],
-        4: [stage_z],
-        5: [stage_heads, stage_wout],
-        6: [stage_heads2],
-        7: [stage_wout2, stage_gathered, call(stage_project, 0, 4)],
-        8: [call(stage_project, 4, 8), stage_norm],
-        9: [stage_up, call(down, 0), call(down, 1), call(scatter, 0)],
+        1: [stage_zgroup],
+        3: [stage_z],
+        4: [stage_heads, stage_wout],
+        5: [stage_heads2, stage_wout2],
+        6: [stage_gathered, call(stage_project, 0, 4)],
+        7: [call(stage_project, 4, 8), stage_norm],
+        8: [stage_up_most],
+        9: [stage_up],
     }
 
     pending = {0: [(0, z)], 1: [(0, z)]}
@@ -590,6 +596,10 @@
                     k = 2 * step - 1 + i
                     send_y(u, k, zk)
                     fresh.append((k, zk))
+            for k, zk in pending[u]:
+                relay_y(u, k, zk)
+            for k, zk in ended[u]:
+                end_y(u, k, zk)
             for j in range(1):
                 for i in range(2):
                     if 1 <= s <= STEPS - i:
@@ -598,10 +608,6 @@
                         arrive(ref, a2_s.at[i, u, s, j], a2_r.at[i, u, s, j])
                         if s + 1 <= STEPS - i:
                             send_a(u, i, s + 1, zk, j)
-            for k, zk in pending[u]:
-                relay_y(u, k, zk)
-            for k, zk in ended[u]:
-                end_y(u, k, zk)
             ended[u], pending[u] = pending[u], fresh
         for stage in stages.get(t, []):
             stage()
@@ -610,18 +616,17 @@
             lo, hi = marks[-3], marks[-2]
             for cp in sent[lo:hi]:
                 cp.wait_send()
-    down(2)
-    scatter(1)
-    finish(0)
-    scatter(2)
-    finish(1)
-    collect(0)
-    finish(2)
-    collect(1)
-    unpack(0)
-    collect(2)
-    unpack(1)
-    unpack(2)
+    for b in range(NB_CUT + 3):
+        if b < NB_CUT:
+            down(b)
+        if 1 <= b < NB_CUT + 1:
+            scatter(b - 1)
+        if 2 <= b < NB_CUT + 2:
+            finish(b - 2)
+        if 3 <= b:
+            collect(b - 3)
+    for b in range(NB_CUT):
+        ended_batch(b)
     for cp in sent[marks[-2] :]:
         cp.wait_send()
     for d in range(1, Z // G):
@@ -681,12 +686,12 @@
             pltpu.VMEM((HEAD // Y + 16, HEAD), BF16),
             pltpu.VMEM((Z // G, HEAD // Y + 16, HEAD), BF16),
             pltpu.VMEM((HEAD, HEAD), F32),
-            pltpu.VMEM((Z, 128, HEAD), BF16),
-            pltpu.VMEM((Z, 128, HEAD), BF16),
-            pltpu.VMEM((Z, 128, HEAD), F32),
-            pltpu.VMEM((X - 1, Z, 32, HEAD), BF16),
-            pltpu.VMEM((X - 1, Z, 32, HEAD), BF16),
-            pltpu.VMEM((C, X, Z, 32, HEAD), BF16),
+            pltpu.VMEM((128, D), BF16),
+            pltpu.VMEM((128, D), BF16),
+            pltpu.VMEM((128, D), F32),
+            pltpu.VMEM((X - 1, 32, D), BF16),
+            pltpu.VMEM((X - 1, 32, D), BF16),
+            pltpu.VMEM((5, ROWS, 256), F32),
             pltpu.SemaphoreType.REGULAR((3,)),
             dma((14,)),
             dma((2, Y)),

time: 102 us -> 98.6 us (0.967)
  Pallas kernels: 99.5 us -> 96.2 us
    pallas_call x1, Pallas kernels: 99.5 us -> 96.2 us  [body(): call(resid, read_pre, keep_pre, written, emit_pre, shrink, floor_c.reshap...]
where the time goes in v3:
time: 98.6 us; the launch traced here: 98.5 us
  Pallas kernels  96.2 us (98%)
  local copies, waits for them, and re-layouts  2.3 us (2%)
    pallas_call x1, Pallas kernels, body(): call(resid, read_pre, keep_pre, written, emit_pre, shrink, floor_c.reshap...  96.2 us
    unnamed x1, local copies, waits for them, and re-layouts  2.3 us

profile of v3, /device:TPU:1, one launch (start us, length us, event | category | flops | bytes accessed | tf_op | source)
XLA Modules:
  0.0 98.5 jit_solution(3661776497003694423)
XLA Ops:
  0.0 96.2 %layer.1 = bf16[256,2048]{1,0:T(8,128)(2,1)} custom-call(bf16[256,2048]{1,0:T(8,128)(2,1)} %resid_in.1, bf16[256,128]{1,0:T(8,128)(2,1)} %read_in.1, bf16[256,128]{1,0:T(8,128)(2,1)} %keep_in.1, bf16[256,128]{1,0:T(8,128)(2,1)} %written_in.1, bf16[256,128]{1,0:T(8,128)(2,1)} %emit_in.1, f32[256,128]{1,0:T(8,128)} %shrink_in.1, f32[1,128]{1,0:T(1,128)} %bitcast.4, ...), custom_call_target="tpu_custom_call" | custom-call | tf_op jit(solution)/shard_map/layer/pallas_call | solution.py:737
  96.2 2.3 %copy.14 = bf16[256,2048]{1,0:T(8,128)(2,1)} copy(bf16[256,2048]{1,0:T(8,128)(2,1)} %layer.1) | data formatting | bytes 2097152
